TPU v7x, 256 devices: a whole 4x4x8 slice. The times are simulated.
256 devices in a mesh: fs: 64 (over z, y, core), tp: 4 (over x).
Axes of the slice: x: 4, y: 4, z: 8, core: 2. Of those that a mesh axis runs over, the one named last changes fastest.
Arguments:
- tokens: bfloat16 [65536, 2048], P('fs', 'tp'), may hold values from -6 to 6
- norm_gain: float32 [2048], P('fs'), may hold values from 0.1 to 1.9
- up_master: float32 [2048, 4096], P('fs', 'tp'), may hold values from -0.125 to 0.125
- down_master: float32 [4096, 2048], P('fs', 'tp'), may hold values from -0.09375 to 0.09375
Outputs:
- mixed: bfloat16 [65536, 2048], P('fs', 'tp')
- up_ready: bfloat16 [2048, 4096], P(None, 'tp')
- down_ready: bfloat16 [4096, 2048], P('tp')
All inputs are finite; a program needn't handle non-finite values.
Results may differ from a plain program's by a relative error of at most 0.0095.
Values may be sent and summed in bfloat16 or wider, within the bound.
A program may use at most 128 MiB of HBM per device.

v0:
```python
import jax
import jax.numpy as jnp
from jax import lax
from jax.sharding import Mesh
from jax.sharding import PartitionSpec as P

FS = ("fs_0", "fs_1", "fs_2")


def sent_to_all(shard, axis):
    peers = lax.axis_size(axis)
    return lax.all_to_all(
        jnp.broadcast_to(shard[None], (peers, *shard.shape)), axis, 0, 0, tiled=True
    )


def laid_out(pieces, dim):
    lengths = list(pieces.shape[1:])
    lengths[dim] *= pieces.shape[0]
    return jnp.moveaxis(pieces, 0, dim).reshape(lengths)


def gathered_by_axis(shard, axes, dim):
    far, near = axes
    initial = sent_to_all(shard, far)
    pieces = jnp.swapaxes(sent_to_all(initial, near), 0, 1)
    return laid_out(pieces.reshape(-1, *shard.shape), dim)


def gather_directly(shard, axis, dim):
    return laid_out(sent_to_all(shard, axis), dim)


def shards(tokens, norm_gain, up_master, down_master):
    group_size = lax.axis_size("tp")
    group_index = lax.axis_index("tp")
    up_local = (norm_gain[:, None] * up_master).astype(jnp.bfloat16)
    up_ready = gathered_by_axis(up_local, (("fs_0", "fs_1"), "fs_2"), 0)
    down_local = down_master.astype(jnp.bfloat16)
    wide_rows = lax.all_gather(down_local, "tp", axis=1, tiled=True)
    whole_down = lax.all_gather(wide_rows, FS, axis=0, tiled=True)
    row_count = whole_down.shape[0] // group_size
    down_ready = lax.dynamic_slice_in_dim(whole_down, group_index * row_count, row_count, 0)
    features = gather_directly(tokens, "tp", 1)
    values = features.astype(jnp.float32)
    mean_square = jnp.mean(values * values, axis=-1, keepdims=True)
    normed = (values * lax.rsqrt(mean_square + 1e-06)).astype(jnp.bfloat16)
    before = jnp.dot(normed, up_ready, preferred_element_type=jnp.float32)
    hidden = jnp.square(jax.nn.relu(before)).astype(jnp.bfloat16)
    partial_value = jnp.dot(hidden, down_ready, preferred_element_type=jnp.float32)
    mixed = lax.psum_scatter(
        partial_value.astype(jnp.bfloat16), "tp", scatter_dimension=1, tiled=True
    )
    return (mixed, up_ready, down_ready)


def solution(mesh):
    finer = Mesh(mesh.devices.reshape(8, 4, 2, mesh.shape["tp"]), ("fs_0", "fs_1", "fs_2", "tp"))
    placed = (P(FS, "tp"), P(FS), P(FS, "tp"), P(FS, "tp"))
    return jax.shard_map(
        shards,
        mesh=finer,
        in_specs=placed,
        out_specs=(P(FS, "tp"), P(None, "tp"), P("tp", None)),
        check_vma=False,
    )
```

profile of v0, /device:TPU:1, one launch (start us, length us, event | category | flops | bytes accessed | tf_op | source)
XLA Modules:
  0.0 243.9 jit_solution(11935646034167226579)
XLA Ops:
  7.2 0.0 all-gather.2.cloned.1.call-start
  7.2 0.9 convert_element_type.33
  8.1 11.8 %all_gather.6 = bf16[64,2048]{1,0:T(8,128)(2,1)} all-gather(bf16[64,512]{1,0:T(8,128)(2,1)S(1)} %convert_element_type.33), channel_id=1, replica_groups=mesh['fs_0'=8,'fs_1'=4,'fs_2'=2,'tp'=4] {'tp'}, dimensions={1}, use_global_device_ids=true | all-gather | bytes 327680 | tf_op jit(solution)/shard_map/all_gather | solution.py:40
  19.9 0.0 all-gather.2.cloned.1.call-update
  20.0 1.5 copy.9
  21.5 2.6 %broadcast_in_dim.6 = bf16[4,1024,512]{1,2,0:T(8,128)(2,1)} broadcast(bf16[1024,512]{0,1:T(8,128)(2,1)S(1)} %copy.9), dimensions={1,2} | broadcast | bytes 5242880 | tf_op jit(solution)/shard_map/broadcast_in_dim | solution.py:13
  24.0 0.0 copy-start
  24.0 0.0 copy-start.1
  24.0 5.0 %all-to-all-start = ((bf16[4,1024,512]{1,2,0:T(8,128)(2,1)}), bf16[4,1024,512]{1,2,0:T(8,128)(2,1)}, u32[]{:S(2)}, u32[]{:S(2)}) async-start(bf16[4,1024,512]{1,2,0:T(8,128)(2,1)} %broadcast_in_dim.6), calls=%async_computation | async-start | bytes 8388608 | tf_op jit(solution)/shard_map/all_to_all | solution.py:12
  29.0 0.0 copy-done
  29.0 0.0 copy-done.1
  29.0 0.1 multiply_convert_fusion.1
  29.1 44.2 %all-to-all-done = bf16[4,1024,512]{1,2,0:T(8,128)(2,1)} async-done(((bf16[4,1024,512]{1,2,0:T(8,128)(2,1)}), bf16[4,1024,512]{1,2,0:T(8,128)(2,1)}, u32[]{:S(2)}, u32[]{:S(2)}) %all-to-all-start) | async-done | bytes 4194336 | tf_op jit(solution)/shard_map/all_to_all | solution.py:12
  73.4 1.6 broadcast_in_dim.7
  74.9 12.8 %all-to-all-start.1 = ((bf16[32,32,1024]{2,1,0:T(8,128)(2,1)}), bf16[32,32,1024]{2,1,0:T(8,128)(2,1)S(1)}, u32[]{:S(2)}, u32[]{:S(2)}) async-start(bf16[32,32,1024]{2,1,0:T(8,128)(2,1)} %broadcast_in_dim.7), calls=%async_computation.1 | async-start | bytes 4194304 | tf_op jit(solution)/shard_map/all_to_all | solution.py:12
  87.7 0.0 reduce-scatter.2.cloned.1.call-start
  87.8 3.2 %fusion = f32[1024]{0:T(1024)S(1)} fusion(bf16[4,1024,512]{1,2,0:T(8,128)(2,1)} %all-to-all-done), kind=kLoop, calls=%fused_computation.2 | loop fusion | flops 6290432 | bytes 4198400 | tf_op jit(solution)/shard_map/reduce_sum | solution.py:46
  91.0 5.5 %fusion.1 = bf16[4,1024,512]{1,2,0:T(8,128)(2,1)} fusion(bf16[4,1024,512]{1,2,0:T(8,128)(2,1)} %all-to-all-done, f32[1024]{0:T(1024)S(1)} %add_rsqrt_fusion), kind=kLoop, calls=%fused_computation.3 | loop fusion | flops 6291456 | bytes 8392704 | tf_op jit(solution)/shard_map/convert_element_type | solution.py:47
  96.5 61.2 %all-to-all-done.1 = bf16[32,32,1024]{2,1,0:T(8,128)(2,1)S(1)} async-done(((bf16[32,32,1024]{2,1,0:T(8,128)(2,1)}), bf16[32,32,1024]{2,1,0:T(8,128)(2,1)S(1)}, u32[]{:S(2)}, u32[]{:S(2)}) %all-to-all-start.1) | async-done | bytes 2097184 | tf_op jit(solution)/shard_map/all_to_all | solution.py:12
  157.6 0.5 broadcast_in_dim.8
  158.2 13.2 %all_to_all.15 = bf16[2,32,32,1024]{3,2,1,0:T(8,128)(2,1)S(1)} all-to-all(bf16[2,32,32,1024]{3,2,1,0:T(8,128)(2,1)S(1)} %broadcast_in_dim.8), channel_id=1, replica_groups=mesh['fs_0'=8,'fs_1'=4,'fs_2'=2,'tp'=4] {'fs_2'}, dimensions={0} | all-to-all | bytes 8388608 | tf_op jit(solution)/shard_map/all_to_all | solution.py:12
  171.4 2.5 %copy.10 = bf16[2,32,32,1024]{3,2,0,1:T(8,128)(2,1)} copy(bf16[2,32,32,1024]{3,2,1,0:T(8,128)(2,1)S(1)} %all_to_all.15) | data formatting | bytes 8388608 | tf_op jit(solution)/shard_map/all_to_all | solution.py:12
  173.9 0.0 all-gather.2.cloned.1.call-done
  173.9 4.8 %constant_dynamic-slice_fusion = bf16[1024,2048]{1,0:T(8,128)(2,1)} fusion(bf16[4096,2048]{1,0:T(8,128)(2,1)} %all-gather.2.cloned.1.call-done, s32[]{:T(128)S(6)} %select_n.3), kind=kLoop, calls=%fused_computation.8 | loop fusion | bytes 8388612 | tf_op jit(solution)/shard_map/dynamic_slice | solution.py:43
  178.6 14.4 %convolution_convert_fusion = bf16[1024,2048]{1,0:T(8,128)(2,1)} fusion(bf16[1024,2048]{1,0:T(8,128)(2,1)} %constant_dynamic-slice_fusion, bf16[1024,2048]{0,1:T(8,128)(2,1)} %bitcast.11, bf16[2048,1024]{1,0:T(8,128)(2,1)} %bitcast.9), kind=kOutput, calls=%fused_computation.5 | convolution fusion | flops 8595177472 | bytes 16777216 | tf_op jit(solution)/shard_map/dot_general | solution.py:50
  193.0 0.0 reduce-scatter.2.cloned.1.call-update
  193.1 44.0 %reduce-scatter.2.cloned.1.call-done = bf16[1024,512]{1,0:T(8,128)(2,1)} async-done(((bf16[1024,2048]{1,0:T(8,128)(2,1)}), bf16[1024,512]{1,0:T(8,128)(2,1)}) %reduce-scatter.2.cloned.1.call-update) | async-done | bytes 1048592 | tf_op jit(solution)/shard_map/reduce_scatter | solution.py:51
  (1 shorter events, 0.0 us)
Async XLA Ops:
  7.2 166.7 %all-gather.2.cloned.1.call-start = ((), (), s32[]{:S(2)}) async-start(), calls=%async_computation.4 | async-start | bytes 17039360 | tf_op jit(solution)/shard_map/all_gather | solution.py:41
  24.0 5.0 %copy-start = (f32[32,1024]{1,0:T(8,128)S(1)}, f32[32,1024]{1,0:T(8,128)}, u32[]{:S(2)}) copy-start(f32[32,1024]{1,0:T(8,128)} %param.6) | copy-start | bytes 393220
  24.0 5.0 %copy-start.1 = (f32[32]{0:T(128)S(1)}, f32[32]{0:T(128)}, u32[]{:S(2)}) copy-start(f32[32]{0:T(128)} %param.5) | copy-start | bytes 388
  24.0 49.3 %all-to-all-start = ((bf16[4,1024,512]{1,2,0:T(8,128)(2,1)}), bf16[4,1024,512]{1,2,0:T(8,128)(2,1)}, u32[]{:S(2)}, u32[]{:S(2)}) async-start(bf16[4,1024,512]{1,2,0:T(8,128)(2,1)} %broadcast_in_dim.6), calls=%async_computation | async-start | bytes 8388608 | tf_op jit(solution)/shard_map/all_to_all | solution.py:12
  74.9 82.7 %all-to-all-start.1 = ((bf16[32,32,1024]{2,1,0:T(8,128)(2,1)}), bf16[32,32,1024]{2,1,0:T(8,128)(2,1)S(1)}, u32[]{:S(2)}, u32[]{:S(2)}) async-start(bf16[32,32,1024]{2,1,0:T(8,128)(2,1)} %broadcast_in_dim.7), calls=%async_computation.1 | async-start | bytes 4194304 | tf_op jit(solution)/shard_map/all_to_all | solution.py:12
  87.7 149.3 %reduce-scatter.2.cloned.1.call-start = ((), (), s32[]{:S(2)}) async-start(), calls=%async_computation.5 | async-start | bytes 5242880 | tf_op jit(solution)/shard_map/reduce_scatter | solution.py:51
Sparse Core Ops, SparseCore 0:
  20.1 148.1 all-gather.1
  193.2 43.8 reduce-scatter.1
where the time goes:
time: 244 us
  waiting for transfers between devices  149 us (61%)
  blocking collectives  25.1 us (10%)
  starting transfers between devices  17.9 us (7%)
  matrix products  14.4 us (6%)
  between operations  14.1 us (6%)
  local copies, waits for them, and re-layouts  13.4 us (5%)
  other arithmetic  9.67 us (4%)
    all_to_all x2, waiting for transfers between devices, sent_to_all(): lax.all_to_all(jnp.broadcast_to(shard[None], (peers, *shard.shape)), axis...  105 us
    reduce_scatter x1, waiting for transfers between devices, shards(): lax.psum_scatter(partial_value.astype(jnp.bfloat16), 'tp', scatter_dimens...  44 us
    all_to_all x2, starting transfers between devices, sent_to_all(): lax.all_to_all(jnp.broadcast_to(shard[None], (peers, *shard.shape)), axis...  17.8 us
    dot_general x1, matrix products, shards(): jnp.dot(hidden, down_ready, preferred_element_type=jnp.float32)  14.4 us
    all_to_all x1, blocking collectives, sent_to_all(): lax.all_to_all(jnp.broadcast_to(shard[None], (peers, *shard.shape)), axis...  13.2 us
    all_gather x1, blocking collectives, shards(): wide_rows = lax.all_gather(down_local, 'tp', axis=1, tiled=True)  11.8 us
    convert_element_type x1, other arithmetic, shards(): normed = (values * lax.rsqrt(mean_square + 1e-06)).astype(jnp.bfloat16)  5.48 us
  transfers between devices with their start and end apart: 4, of which 3 were waited for; matrix products, arithmetic and copies ran while one was open for 7% of the time, Pallas kernels for 0%

commit v1 on v0

--- a/solution.py
+++ b/solution.py
@@ -37,7 +37,9 @@
     up_local = (norm_gain[:, None] * up_master).astype(jnp.bfloat16)
     up_ready = gathered_by_axis(up_local, (("fs_0", "fs_1"), "fs_2"), 0)
     down_local = down_master.astype(jnp.bfloat16)
-    wide_rows = lax.all_gather(down_local, "tp", axis=1, tiled=True)
+    wide_rows = jnp.concatenate(
+        lax.all_to_all(jnp.stack([down_local] * lax.axis_size("tp")), "tp", 0, 0), axis=1
+    )
     whole_down = lax.all_gather(wide_rows, FS, axis=0, tiled=True)
     row_count = whole_down.shape[0] // group_size
     down_ready = lax.dynamic_slice_in_dim(whole_down, group_index * row_count, row_count, 0)

time: 244 us -> 244 us (level)
  waiting for transfers between devices: 149 us -> 153 us
  blocking collectives: 25.1 us -> 21.5 us
    all_gather x1 -> x0, blocking collectives: 11.8 us -> none  [shards(): wide_rows = lax.all_gather(down_local, 'tp', axis=1, tiled=True)]
    all_to_all x0 -> x1, blocking collectives: none -> 10.2 us  [shards(): lax.all_to_all(jnp.stack([down_local] * lax.axis_size('tp')), 'tp', 0, 0)]
    all_to_all x2, waiting for transfers between devices: 105 us -> 110 us  [sent_to_all(): lax.all_to_all(jnp.broadcast_to(shard[None], (peers, *shard.shape)), axis...]
where the time goes in v1:
time: 244 us; the launch traced here: 243 us
  waiting for transfers between devices  153 us (63%)
  blocking collectives  21.5 us (9%)
  starting transfers between devices  16.3 us (7%)
  matrix products  14.4 us (6%)
  local copies, waits for them, and re-layouts  14.1 us (6%)
  between operations  14.1 us (6%)
  other arithmetic  9.58 us (4%)
    all_to_all x2, waiting for transfers between devices, sent_to_all(): lax.all_to_all(jnp.broadcast_to(shard[None], (peers, *shard.shape)), axis...  110 us
    reduce_scatter x1, waiting for transfers between devices, shards(): lax.psum_scatter(partial_value.astype(jnp.bfloat16), 'tp', scatter_dimens...  43.6 us
    all_to_all x2, starting transfers between devices, sent_to_all(): lax.all_to_all(jnp.broadcast_to(shard[None], (peers, *shard.shape)), axis...  16.2 us
    dot_general x1, matrix products, shards(): jnp.dot(hidden, down_ready, preferred_element_type=jnp.float32)  14.4 us
    all_to_all x1, blocking collectives, sent_to_all(): lax.all_to_all(jnp.broadcast_to(shard[None], (peers, *shard.shape)), axis...  11.3 us
    all_to_all x1, blocking collectives, shards(): lax.all_to_all(jnp.stack([down_local] * lax.axis_size('tp')), 'tp', 0, 0)  10.2 us
    convert_element_type x1, other arithmetic, shards(): normed = (values * lax.rsqrt(mean_square + 1e-06)).astype(jnp.bfloat16)  5.44 us
  transfers between devices with their start and end apart: 4, of which 3 were waited for; matrix products, arithmetic and copies ran while one was open for 7% of the time, Pallas kernels for 0%

profile of v1, /device:TPU:1, one launch (start us, length us, event | category | flops | bytes accessed | tf_op | source)
XLA Modules:
  0.0 243.3 jit_solution(8823815695074514513)
XLA Ops:
  7.2 0.0 all-gather.2.cloned.1.call-start
  7.2 0.9 convert_element_type.33
  8.2 10.2 %all_to_all.20 = bf16[4,64,512]{2,1,0:T(8,128)(2,1)S(1)} all-to-all(bf16[4,64,512]{2,1,0:T(8,128)(2,1)S(1)} %stack.2), channel_id=1, replica_groups=mesh['fs_0'=8,'fs_1'=4,'fs_2'=2,'tp'=4] {'tp'}, dimensions={0} | all-to-all | bytes 524288 | tf_op jit(solution)/shard_map/all_to_all | solution.py:41
  18.3 0.7 copy.12
  19.1 0.0 all-gather.2.cloned.1.call-update
  19.1 1.5 copy.9
  20.6 2.6 %broadcast_in_dim.6 = bf16[4,1024,512]{1,2,0:T(8,128)(2,1)} broadcast(bf16[1024,512]{0,1:T(8,128)(2,1)S(1)} %copy.9), dimensions={1,2} | broadcast | bytes 5242880 | tf_op jit(solution)/shard_map/broadcast_in_dim | solution.py:13
  23.1 0.0 copy-start
  23.2 0.0 copy-start.1
  23.2 5.0 %all-to-all-start = ((bf16[4,1024,512]{1,2,0:T(8,128)(2,1)}), bf16[4,1024,512]{1,2,0:T(8,128)(2,1)}, u32[]{:S(2)}, u32[]{:S(2)}) async-start(bf16[4,1024,512]{1,2,0:T(8,128)(2,1)} %broadcast_in_dim.6), calls=%async_computation | async-start | bytes 8388608 | tf_op jit(solution)/shard_map/all_to_all | solution.py:12
  28.1 0.0 copy-done
  28.1 0.0 copy-done.1
  28.2 0.1 multiply_convert_fusion.1
  28.2 46.8 %all-to-all-done = bf16[4,1024,512]{1,2,0:T(8,128)(2,1)} async-done(((bf16[4,1024,512]{1,2,0:T(8,128)(2,1)}), bf16[4,1024,512]{1,2,0:T(8,128)(2,1)}, u32[]{:S(2)}, u32[]{:S(2)}) %all-to-all-start) | async-done | bytes 4194336 | tf_op jit(solution)/shard_map/all_to_all | solution.py:12
  75.0 1.6 broadcast_in_dim.7
  76.6 11.2 %all-to-all-start.1 = ((bf16[32,32,1024]{2,1,0:T(8,128)(2,1)}), bf16[32,32,1024]{2,1,0:T(8,128)(2,1)S(1)}, u32[]{:S(2)}, u32[]{:S(2)}) async-start(bf16[32,32,1024]{2,1,0:T(8,128)(2,1)} %broadcast_in_dim.7), calls=%async_computation.1 | async-start | bytes 4194304 | tf_op jit(solution)/shard_map/all_to_all | solution.py:12
  87.8 0.0 reduce-scatter.2.cloned.1.call-start
  87.9 3.1 %fusion = f32[1024]{0:T(1024)S(1)} fusion(bf16[4,1024,512]{1,2,0:T(8,128)(2,1)} %all-to-all-done), kind=kLoop, calls=%fused_computation.2 | loop fusion | flops 6290432 | bytes 4198400 | tf_op jit(solution)/shard_map/reduce_sum | solution.py:48
  91.0 5.4 %fusion.1 = bf16[4,1024,512]{1,2,0:T(8,128)(2,1)} fusion(bf16[4,1024,512]{1,2,0:T(8,128)(2,1)} %all-to-all-done, f32[1024]{0:T(1024)S(1)} %add_rsqrt_fusion), kind=kLoop, calls=%fused_computation.3 | loop fusion | flops 6291456 | bytes 8392704 | tf_op jit(solution)/shard_map/convert_element_type | solution.py:49
  96.4 62.9 %all-to-all-done.1 = bf16[32,32,1024]{2,1,0:T(8,128)(2,1)S(1)} async-done(((bf16[32,32,1024]{2,1,0:T(8,128)(2,1)}), bf16[32,32,1024]{2,1,0:T(8,128)(2,1)S(1)}, u32[]{:S(2)}, u32[]{:S(2)}) %all-to-all-start.1) | async-done | bytes 2097184 | tf_op jit(solution)/shard_map/all_to_all | solution.py:12
  159.4 0.5 broadcast_in_dim.8
  159.9 11.3 %all_to_all.21 = bf16[2,32,32,1024]{3,2,1,0:T(8,128)(2,1)S(1)} all-to-all(bf16[2,32,32,1024]{3,2,1,0:T(8,128)(2,1)S(1)} %broadcast_in_dim.8), channel_id=1, replica_groups=mesh['fs_0'=8,'fs_1'=4,'fs_2'=2,'tp'=4] {'fs_2'}, dimensions={0} | all-to-all | bytes 8388608 | tf_op jit(solution)/shard_map/all_to_all | solution.py:12
  171.2 2.5 %copy.10 = bf16[2,32,32,1024]{3,2,0,1:T(8,128)(2,1)} copy(bf16[2,32,32,1024]{3,2,1,0:T(8,128)(2,1)S(1)} %all_to_all.21) | data formatting | bytes 8388608 | tf_op jit(solution)/shard_map/all_to_all | solution.py:12
  173.7 0.0 all-gather.2.cloned.1.call-done
  173.7 4.8 %constant_dynamic-slice_fusion = bf16[1024,2048]{1,0:T(8,128)(2,1)} fusion(bf16[4096,2048]{1,0:T(8,128)(2,1)} %all-gather.2.cloned.1.call-done, s32[]{:T(128)S(6)} %select_n.3), kind=kLoop, calls=%fused_computation.8 | loop fusion | bytes 8388612 | tf_op jit(solution)/shard_map/dynamic_slice | solution.py:45
  178.5 14.4 %convolution_convert_fusion = bf16[1024,2048]{1,0:T(8,128)(2,1)} fusion(bf16[1024,2048]{1,0:T(8,128)(2,1)} %constant_dynamic-slice_fusion, bf16[1024,2048]{0,1:T(8,128)(2,1)} %bitcast.14, bf16[2048,1024]{1,0:T(8,128)(2,1)} %bitcast.12), kind=kOutput, calls=%fused_computation.5 | convolution fusion | flops 8595177472 | bytes 16777216 | tf_op jit(solution)/shard_map/dot_general | solution.py:52
  192.9 0.0 reduce-scatter.2.cloned.1.call-update
  192.9 43.6 %reduce-scatter.2.cloned.1.call-done = bf16[1024,512]{1,0:T(8,128)(2,1)} async-done(((bf16[1024,2048]{1,0:T(8,128)(2,1)}), bf16[1024,512]{1,0:T(8,128)(2,1)}) %reduce-scatter.2.cloned.1.call-update) | async-done | bytes 1048592 | tf_op jit(solution)/shard_map/reduce_scatter | solution.py:53
  (2 shorter events, 0.0 us)
Async XLA Ops:
  7.2 166.5 %all-gather.2.cloned.1.call-start = ((), (), s32[]{:S(2)}) async-start(), calls=%async_computation.5 | async-start | bytes 17039360 | tf_op jit(solution)/shard_map/all_gather | solution.py:43
  23.1 5.0 %copy-start = (f32[32,1024]{1,0:T(8,128)S(1)}, f32[32,1024]{1,0:T(8,128)}, u32[]{:S(2)}) copy-start(f32[32,1024]{1,0:T(8,128)} %param.6) | copy-start | bytes 393220
  23.2 5.0 %copy-start.1 = (f32[32]{0:T(128)S(1)}, f32[32]{0:T(128)}, u32[]{:S(2)}) copy-start(f32[32]{0:T(128)} %param.5) | copy-start | bytes 388
  23.2 51.9 %all-to-all-start = ((bf16[4,1024,512]{1,2,0:T(8,128)(2,1)}), bf16[4,1024,512]{1,2,0:T(8,128)(2,1)}, u32[]{:S(2)}, u32[]{:S(2)}) async-start(bf16[4,1024,512]{1,2,0:T(8,128)(2,1)} %broadcast_in_dim.6), calls=%async_computation | async-start | bytes 8388608 | tf_op jit(solution)/shard_map/all_to_all | solution.py:12
  76.6 82.8 %all-to-all-start.1 = ((bf16[32,32,1024]{2,1,0:T(8,128)(2,1)}), bf16[32,32,1024]{2,1,0:T(8,128)(2,1)S(1)}, u32[]{:S(2)}, u32[]{:S(2)}) async-start(bf16[32,32,1024]{2,1,0:T(8,128)(2,1)} %broadcast_in_dim.7), calls=%async_computation.1 | async-start | bytes 4194304 | tf_op jit(solution)/shard_map/all_to_all | solution.py:12
  87.8 148.7 %reduce-scatter.2.cloned.1.call-start = ((), (), s32[]{:S(2)}) async-start(), calls=%async_computation.6 | async-start | bytes 5242880 | tf_op jit(solution)/shard_map/reduce_scatter | solution.py:53
Sparse Core Ops, SparseCore 0:
  19.2 147.1 all-gather.1
  193.0 43.3 reduce-scatter.1
